TPU v7x, 32 devices: a whole 2x2x4 slice. The times are simulated.
32 devices in a mesh: grp: 2 (over x), ep: 16 (over z, y, core).
Axes of the slice: x: 2, y: 2, z: 4, core: 2. Of those that a mesh axis runs over, the one named last changes fastest.
Arguments:
- tokens: bfloat16 [8192, 2048], P(('grp', 'ep')), parts along dimension 0, may hold values from -6 to 6
- norm_gain: float32 [2048], replicated, may hold values from 0.1 to 1.9
- routes: int32 [8192, 2], P(('grp', 'ep')), parts along dimension 0, may hold values from 0 to 15, all different within a row; in each aligned block of 256 rows (0 to 255, 256 to 511, ...) at most 40 rows name the same one
- route_weights: float32 [8192, 2], P(('grp', 'ep')), parts along dimension 0, may hold values from 0.2 to 1.5
- expert_gate: bfloat16 [16, 2048, 256], P('ep'), may hold values from -0.125 to 0.125
- expert_up: bfloat16 [16, 2048, 256], P('ep'), may hold values from -0.125 to 0.125
- expert_down: bfloat16 [16, 256, 2048], P('ep'), may hold values from -0.375 to 0.375
- shared_gate: bfloat16 [2048, 256], replicated, may hold values from -0.125 to 0.125
- shared_up: bfloat16 [2048, 256], replicated, may hold values from -0.125 to 0.125
- shared_down: bfloat16 [256, 2048], replicated, may hold values from -0.375 to 0.375
Outputs:
- mixed: bfloat16 [8192, 2048], P(('grp', 'ep')), parts along dimension 0
There are 2 independent parts, one for each index of `grp`. A program takes and returns all parts, laid end to end along the dimension named above; an argument that names none is the same for every part. Nothing has to cross between parts.
Inputs may be any that keep to these rules, and one draw needn't show every extreme that they name: `routes`: the 2 experts of a token are distinct. Among the tokens of one device, at most 40 choose any one expert; in every draw some expert is chosen by exactly 40 tokens of some device.
All inputs are finite; a program needn't handle non-finite values.
Results may differ from a plain program's by a relative error of at most 0.0075.
Values may be sent and summed in bfloat16 or wider, within the bound.
A program may use at most 64 MiB of HBM per device.

v0:
```python
import jax
import jax.numpy as jnp
from jax import lax
from jax.sharding import PartitionSpec as P


def swiglu_rows(row_block, w_gate, w_up, w_down):
    gate_part = jnp.dot(row_block, w_gate, preferred_element_type=jnp.float32)
    up_part = jnp.dot(row_block, w_up, preferred_element_type=jnp.float32)
    hidden = (jax.nn.silu(gate_part) * up_part).astype(jnp.bfloat16)
    return jnp.dot(hidden, w_down, preferred_element_type=jnp.float32)


def on_device(
    tokens,
    norm_gain,
    routes,
    route_weights,
    expert_gate,
    expert_up,
    expert_down,
    shared_gate,
    shared_up,
    shared_down,
):
    tok_rows, model_width = tokens.shape
    top_count = routes.shape[1]
    devices_ep = lax.axis_size("ep")
    capacity = 5 * tok_rows * top_count // (4 * devices_ep)
    upcast = tokens.astype(jnp.float32)
    factor = lax.rsqrt(jnp.mean(upcast * upcast, axis=-1, keepdims=True) + 1e-06)
    normed = (upcast * factor * norm_gain).astype(jnp.bfloat16)
    flat_expert = routes.reshape(-1)
    onehot = (flat_expert[:, None] == jnp.arange(devices_ep, dtype=jnp.int32)[None, :]).astype(
        jnp.int32
    )
    position = jnp.sum(jnp.cumsum(onehot, axis=0) * onehot, axis=1) - 1
    slot_index = flat_expert * capacity + position
    pair_token = jnp.arange(tok_rows * top_count, dtype=jnp.int32) // top_count
    slot_token = (
        jnp.full((devices_ep * capacity,), tok_rows, jnp.int32).at[slot_index].set(pair_token)
    )
    padded = jnp.concatenate([normed, jnp.zeros((1, model_width), jnp.bfloat16)], axis=0)
    outgoing = padded[slot_token].reshape(devices_ep, capacity, model_width)
    arrived = lax.all_to_all(outgoing, "ep", split_axis=0, concat_axis=0, tiled=True)
    flat_rows = arrived.reshape(devices_ep * capacity, model_width)
    expert_rows = swiglu_rows(flat_rows, expert_gate[0], expert_up[0], expert_down[0]).astype(
        jnp.bfloat16
    )
    returned = lax.all_to_all(
        expert_rows.reshape(devices_ep, capacity, model_width),
        "ep",
        split_axis=0,
        concat_axis=0,
        tiled=True,
    )
    pair_out = returned.reshape(devices_ep * capacity, model_width)[slot_index]
    pair_out = pair_out.reshape(tok_rows, top_count, model_width)
    routed = jnp.einsum("tk,tkd->td", route_weights, pair_out.astype(jnp.float32))
    shared_result = swiglu_rows(normed, shared_gate, shared_up, shared_down)
    return (routed + shared_result).astype(jnp.bfloat16)


def solution(mesh):
    return jax.shard_map(
        on_device,
        mesh=mesh,
        in_specs=(
            P(("grp", "ep"), None),
            P(),
            P(("grp", "ep"), None),
            P(("grp", "ep"), None),
            P("ep", None, None),
            P("ep", None, None),
            P("ep", None, None),
            P(),
            P(),
            P(),
        ),
        out_specs=P(("grp", "ep"), None),
        check_vma=False,
    )
```

profile of v0, /device:TPU:13, one launch (start us, length us, event | category | flops | bytes accessed | tf_op | source)
XLA Modules:
  0.0 173.6 jit_solution(4842441966873378192)
XLA Ops:
  0.0 1.0 copy.12
  1.0 0.1 eq.29
  1.1 0.1 eq.25
  1.3 0.7 broadcast_multiply_fusion
  2.0 1.2 reduce-window.6
  3.1 0.2 slice_reduce_fusion
  3.5 0.1 copy.11
  3.6 0.1 mul.59
  3.8 2.4 %scatter_custom_fusion = s32[640]{0:T(1024)S(1)} fusion(s32[512]{0:T(512)S(1)} %bitcast.45, s32[512]{0:T(512)S(1)} %add_select_fusion, s32[]{:T(128)} %constant.39.clone.1), kind=kCustom, calls=%fused_computation.49 | custom fusion | bytes 2564 | tf_op jit(solution)/shard_map/scatter | solution.py:41
  6.3 1.5 fusion.1
  7.8 1.0 fusion.3
  8.8 0.1 concatenate.3
  8.9 4.1 %gather_fusion = bf16[640,2048]{1,0:T(8,128)(2,1)} fusion(bf16[257,2048]{1,0:T(8,128)(2,1)S(1)} %concatenate.3, s32[1024]{0:T(1024)S(1)} %pad_clamp_fusion.1), kind=kCustom, calls=%fused_computation | custom fusion | bytes 5245440 | tf_op jit(solution)/shard_map/gather | solution.py:44
  13.0 65.3 %all_to_all.10 = bf16[16,40,2048]{2,1,0:T(8,128)(2,1)} all-to-all(bf16[16,40,2048]{2,1,0:T(8,128)(2,1)} %bitcast.43), channel_id=1, replica_groups=mesh['grp'=2,'ep'=16] {'ep'}, dimensions={0} | all-to-all | bytes 5242880 | tf_op jit(solution)/shard_map/all_to_all | solution.py:45
  78.3 3.4 %fusion.9 = f32[640,256]{1,0:T(8,128)} fusion(bf16[640,2048]{1,0:T(8,128)(2,1)} %bitcast.4, bf16[1,2048,256]{2,1,0:T(8,128)(2,1)S(1)} %copy-done.5), kind=kOutput, calls=%fused_computation.17 | convolution fusion | flops 671088640 | bytes 4325376 | tf_op jit(solution)/shard_map/dot_general | solution.py:8
  81.7 6.5 %convolution_convert_fusion = bf16[640,2048]{1,0:T(8,128)(2,1)} fusion(bf16[640,2048]{1,0:T(8,128)(2,1)} %bitcast.4, bf16[1,256,2048]{2,1,0:T(8,128)(2,1)S(1)} %copy-done, bf16[1,2048,256]{2,1,0:T(8,128)(2,1)} %param.15, f32[640,256]{1,0:T(8,128)} %fusion.9), kind=kOutput, calls=%fused_computation.3 | convolution fusion | flops 1344471040 | bytes 7995392 | tf_op jit(solution)/shard_map/dot_general | solution.py:11
  88.3 5.2 %all-to-all-start.1 = ((bf16[16,40,2048]{2,1,0:T(8,128)(2,1)}), bf16[16,40,2048]{2,1,0:T(8,128)(2,1)}, u32[]{:S(2)}, u32[]{:S(2)}) async-start(bf16[16,40,2048]{2,1,0:T(8,128)(2,1)} %bitcast.44), calls=%async_computation.1 | async-start | bytes 5242880 | tf_op jit(solution)/shard_map/all_to_all | solution.py:50
  93.5 0.2 copy.15
  93.7 0.4 fusion.34
  94.1 58.1 %all-to-all-done.1 = bf16[16,40,2048]{2,1,0:T(8,128)(2,1)} async-done(((bf16[16,40,2048]{2,1,0:T(8,128)(2,1)}), bf16[16,40,2048]{2,1,0:T(8,128)(2,1)}, u32[]{:S(2)}, u32[]{:S(2)}) %all-to-all-start.1) | async-done | bytes 2621472 | tf_op jit(solution)/shard_map/all_to_all | solution.py:50
  152.2 7.3 %gather_fusion.1 = bf16[512,2048]{1,0:T(8,128)(2,1)} fusion(bf16[640,2048]{1,0:T(8,128)(2,1)} %bitcast.9, s32[1024]{0:T(1024)S(1)} %pad_clamp_fusion), kind=kCustom, calls=%fused_computation.1 | custom fusion | bytes 4196352 | tf_op jit(solution)/shard_map/gather | solution.py:57
  159.5 4.4 %reshape.80 = bf16[256,2,2048]{2,1,0:T(2,128)(2,1)} reshape(bf16[512,2048]{1,0:T(8,128)(2,1)} %gather_fusion.1) | data formatting | bytes 4194304 | tf_op jit(solution)/shard_map/reshape | solution.py:58
  163.9 5.3 %fusion.33 = f32[256,1,2048]{2,1,0:T(1,128)} fusion(bf16[256,2,2048]{2,1,0:T(2,128)(2,1)} %reshape.80, bf16[256,2,1]{1,2,0:T(2,128)(2,1)S(1)} %copy.15), kind=kOutput, calls=%fused_computation.57 | convolution fusion | flops 2097152 | bytes 4195328 | tf_op jit(solution)/shard_map/tk,tkd->td/dot_general | solution.py:59
  169.2 4.4 %fusion = bf16[256,2048]{1,0:T(8,128)(2,1)} fusion(bf16[256,2048]{1,0:T(8,128)(2,1)S(1)} %copy-done.2, f32[256,1,2048]{2,1,0:T(1,128)} %fusion.33, bf16[256,2048]{1,0:T(8,128)(2,1)S(1)} %fusion.3, bf16[2048,256]{1,0:T(8,128)(2,1)} %param.18, f32[256,256]{1,0:T(8,128)S(1)} %fusion.34), kind=kOutput, calls=%fused_computation.7 | convolution fusion | flops 538312704 | bytes 6553600 | tf_op jit(solution)/shard_map/dot_general | solution.py:11
  (23 shorter events, 0.2 us)
Async XLA Ops:
  0.0 81.7 %copy-start = (bf16[1,256,2048]{2,1,0:T(8,128)(2,1)S(1)}, bf16[1,256,2048]{2,1,0:T(8,128)(2,1)}, u32[]{:S(2)}) copy-start(bf16[1,256,2048]{2,1,0:T(8,128)(2,1)} %param.16) | copy-start | bytes 3145732
  0.0 7.8 %copy-start.1 = (bf16[256,2048]{1,0:T(8,128)(2,1)S(1)}, bf16[256,2048]{1,0:T(8,128)(2,1)}, u32[]{:S(2)}) copy-start(bf16[256,2048]{1,0:T(8,128)(2,1)} %param.10) | copy-start | bytes 3145732
  13.0 65.3 %copy-start.5 = (bf16[1,2048,256]{2,1,0:T(8,128)(2,1)S(1)}, bf16[1,2048,256]{2,1,0:T(8,128)(2,1)}, u32[]{:S(2)}) copy-start(bf16[1,2048,256]{2,1,0:T(8,128)(2,1)} %param.14) | copy-start | bytes 3145732
  88.3 5.2 %copy-start.4 = (f32[256,2]{0,1:T(2,128)S(1)}, f32[256,2]{0,1:T(2,128)}, u32[]{:S(2)}) copy-start(f32[256,2]{0,1:T(2,128)} %param.13) | copy-start | bytes 6148
  88.3 5.4 %copy-start.3 = (bf16[2048,256]{1,0:T(8,128)(2,1)S(1)}, bf16[2048,256]{1,0:T(8,128)(2,1)}, u32[]{:S(2)}) copy-start(bf16[2048,256]{1,0:T(8,128)(2,1)} %param.17) | copy-start | bytes 3145732
  88.3 64.0 %all-to-all-start.1 = ((bf16[16,40,2048]{2,1,0:T(8,128)(2,1)}), bf16[16,40,2048]{2,1,0:T(8,128)(2,1)}, u32[]{:S(2)}, u32[]{:S(2)}) async-start(bf16[16,40,2048]{2,1,0:T(8,128)(2,1)} %bitcast.44), calls=%async_computation.1 | async-start | bytes 5242880 | tf_op jit(solution)/shard_map/all_to_all | solution.py:50
  163.9 5.3 %copy-start.2 = (bf16[256,2048]{1,0:T(8,128)(2,1)S(1)}, bf16[256,2048]{1,0:T(8,128)(2,1)}, u32[]{:S(2)}) copy-start(bf16[256,2048]{1,0:T(8,128)(2,1)} %param.19) | copy-start | bytes 3145732
where the time goes:
time: 174 us
  blocking collectives  65.3 us (38%)
  waiting for transfers between devices  58.1 us (33%)
  local copies, waits for them, and re-layouts  20.3 us (12%)
  matrix products  20 us (11%)
  starting transfers between devices  5.19 us (3%)
  other arithmetic  4.53 us (3%)
    all_to_all x1, blocking collectives, on_device(): lax.all_to_all(outgoing, 'ep', split_axis=0, concat_axis=0, tiled=True)  65.3 us
    all_to_all x1, waiting for transfers between devices, on_device(): lax.all_to_all(expert_rows.reshape(devices_ep, capacity, model_width), 'e...  58.1 us
    dot_general x2, matrix products, swiglu_rows(): return jnp.dot(hidden, w_down, preferred_element_type=jnp.float32)  10.9 us
    gather x1, local copies, waits for them, and re-layouts, on_device(): pair_out = returned.reshape(devices_ep * capacity, model_width)[slot_index]  7.29 us
    dot_general x1, matrix products, on_device(): jnp.einsum('tk,tkd->td', route_weights, pair_out.astype(jnp.float32))  5.29 us
    all_to_all x1, starting transfers between devices, on_device(): lax.all_to_all(expert_rows.reshape(devices_ep, capacity, model_width), 'e...  5.19 us
    reshape x1, local copies, waits for them, and re-layouts, on_device(): pair_out = pair_out.reshape(tok_rows, top_count, model_width)  4.4 us
    gather x1, local copies, waits for them, and re-layouts, on_device(): outgoing = padded[slot_token].reshape(devices_ep, capacity, model_width)  4.11 us
  transfers between devices with their start and end apart: 1, of which 1 were waited for; matrix products, arithmetic and copies ran while one was open for 0% of the time, Pallas kernels for 0%

commit v1 on v0

v1 whole, which is shorter than its diff:
```python
import functools

import jax
import jax.numpy as jnp
from jax import lax
from jax.experimental import pallas as pl
from jax.experimental.pallas import tpu as pltpu
from jax.sharding import PartitionSpec as P

BF16 = jnp.bfloat16
F32 = jnp.float32
PIECES = 2


def dot(a, b, dims=((1,), (0,))):
    return lax.dot_general(a, b, (dims, ((), ())), preferred_element_type=F32)


def hidden_rows(rows, w_gate, w_up):
    gate_part = dot(rows, w_gate)
    up_part = dot(rows, w_up)
    return (gate_part / (1.0 + jnp.exp(-gate_part)) * up_part).astype(BF16)


def kernel(
    n, groups, cap,
    tokens_hbm, gain_ref, routes_ref, rw_ref, eg_hbm, eu_hbm, ed_hbm, sg_hbm, su_hbm, sd_hbm,
    out_ref,
    tok, normed, place, scale, wg, wu, wd, fg, fu, fd, sg, su, sd, obuf, arr, ybuf, ret, acc,
    load_sem, wsend, wrecv, xsend, xrecv, dsend, drecv, rsend, rrecv,
):
    half = n // 2
    me = lax.axis_index("ep")
    grp = lax.axis_index("grp")
    base = (me // half) * half
    mine = me % half
    far = (me + half) % n
    rows = tok.shape[0]
    width = tok.shape[1]

    def peer(j):
        total, bit = 0, 1
        while bit < half:
            total = total + bit * (((mine // bit) % 2 + (j // bit) % 2) % 2)
            bit *= 2
        return total

    barrier = pltpu.get_barrier_semaphore()

    def greet(i, c):
        pl.semaphore_signal(barrier, inc=1, device_id={"ep": base + peer(i)})
        return c

    lax.fori_loop(1, half, greet, 0)
    pl.semaphore_signal(barrier, inc=1, device_id={"ep": far})
    for k in range(1, groups):
        pl.semaphore_signal(barrier, inc=1, device_id={"grp": (grp + k) % groups})

    loads = [(tokens_hbm, tok), (eg_hbm.at[0], wg), (eu_hbm.at[0], wu), (ed_hbm.at[0], wd),
             (sg_hbm, sg), (su_hbm, su), (sd_hbm, sd)]
    loads = [pltpu.make_async_copy(a, b, load_sem.at[i]) for i, (a, b) in enumerate(loads)]
    for copy in loads:
        copy.start()

    def share(group, array, piece):
        depth = array.shape[-2] // groups // PIECES
        start = (group * PIECES + piece) * depth
        return pl.ds(pl.multiple_of(start, depth), depth)

    def weight_copy(a, piece):
        src, dst = ((eg_hbm, fg), (eu_hbm, fu), (ed_hbm, fd))[a]
        where = share(grp, dst, piece)
        return pltpu.make_async_remote_copy(
            src_ref=src.at[0, where], dst_ref=dst.at[where],
            send_sem=wsend.at[a * PIECES + piece], recv_sem=wrecv.at[a * PIECES + piece],
            device_id={"ep": far})

    def forward_copy(a, piece, k):
        dst = (fg, fu, fd)[a]
        where = share(grp, dst, piece)
        i = (a * PIECES + piece) * max(1, groups - 1) + k - 1
        return pltpu.make_async_remote_copy(
            src_ref=dst.at[where], dst_ref=dst.at[where],
            send_sem=xsend.at[i], recv_sem=xrecv.at[i],
            device_id={"grp": (grp + k) % groups})

    pl.semaphore_wait(barrier, half - 1 + 1 + groups - 1)
    chunks = [(a, piece) for a in range(3) for piece in range(PIECES)]
    for a, piece in chunks:
        weight_copy(a, piece).start()

    lane = lax.broadcasted_iota(jnp.int32, (rows, 128), 1)
    chosen = jnp.zeros((rows, 128), F32)
    weight = jnp.zeros((rows, 128), F32)
    for k in range(routes_ref.shape[1]):
        hit = lane == routes_ref[:, k:k + 1]
        chosen = chosen + jnp.where(hit, 1.0, 0.0)
        weight = weight + jnp.where(hit, rw_ref[:, k:k + 1], 0.0)
    chosen_t = chosen.T
    earlier = (lax.broadcasted_iota(jnp.int32, (rows, rows), 0)
               < lax.broadcasted_iota(jnp.int32, (rows, rows), 1))
    before = dot(chosen_t.astype(BF16), jnp.where(earlier, 1.0, 0.0).astype(BF16))
    place[...] = jnp.where(chosen_t > 0.5, before, -1.0)
    scale[...] = weight.T

    loads[0].wait()

    def norm_step(i, c):
        at = pl.ds(pl.multiple_of(i * 32, 32), 32)
        x = tok[at, :].astype(F32)
        factor = lax.rsqrt(jnp.mean(x * x, axis=-1, keepdims=True) + 1e-06)
        normed[at, :] = (x * factor * gain_ref[...]).astype(BF16)
        return c

    lax.fori_loop(0, rows // 32, norm_step, 0)
    slot = lax.broadcasted_iota(jnp.int32, (cap, rows), 0).astype(F32)

    def gather(p):
        ours = slot == place[pl.ds(base + p, 1), :]
        theirs = slot == place[pl.ds((base + half) % n + p, 1), :]
        pick = jnp.concatenate([jnp.where(ours, 1.0, 0.0), jnp.where(theirs, 1.0, 0.0)], axis=0)
        got = dot(pick.astype(BF16), normed[...])
        return got[:cap].astype(BF16), got[cap:].astype(BF16)

    def dispatch_copy(p):
        return pltpu.make_async_remote_copy(
            src_ref=obuf.at[p], dst_ref=arr.at[mine],
            send_sem=dsend.at[p], recv_sem=drecv.at[mine], device_id={"ep": base + p})

    def dispatch_wait(p):
        pltpu.make_async_remote_copy(
            src_ref=obuf.at[p], dst_ref=arr.at[p],
            send_sem=dsend.at[p], recv_sem=drecv.at[p], device_id={"ep": base + p}).wait_recv()

    def return_copy(p, b):
        return pltpu.make_async_remote_copy(
            src_ref=ybuf.at[p, b], dst_ref=ret.at[mine, b],
            send_sem=rsend.at[p, b], recv_sem=rrecv.at[mine, b], device_id={"ep": base + p})

    def return_wait(p, b):
        pltpu.make_async_remote_copy(
            src_ref=ybuf.at[p, b], dst_ref=ret.at[p, b],
            send_sem=rsend.at[p, b], recv_sem=rrecv.at[p, b], device_id={"ep": base + p}).wait_recv()

    def dispatch_step(i, c):
        p = peer(half - 1 - i)
        first, second = gather(p)
        obuf[p, 0] = first
        obuf[p, 1] = second
        dispatch_copy(p).start()
        return c

    lax.fori_loop(0, half - 1, dispatch_step, 0)
    first, second = gather(mine)
    arr[mine, 0] = first
    arr[mine, 1] = second

    for copy in loads[4:]:
        copy.wait()
    acc[...] = dot(hidden_rows(normed[...], sg[...], su[...]), sd[...])
    for copy in loads[1:4]:
        copy.wait()

    def combine(p, b):
        e = (base + b * half) % n + p
        pick = jnp.where(slot == place[pl.ds(e, 1), :], scale[pl.ds(e, 1), :], 0.0)
        acc[...] += dot(pick.astype(BF16), ret[p, b], ((0,), (0,)))

    def own_step(i, c):
        p = peer(half - 1 - i)
        dispatch_wait(p)
        ybuf[p, 0] = dot(hidden_rows(arr[p, 0], wg[...], wu[...]), wd[...]).astype(BF16)
        return_copy(p, 0).start()
        return c

    def forward(a, piece):
        weight_copy(a, piece).wait_recv()
        for k in range(1, groups):
            forward_copy(a, piece, k).start()

    done = 0
    for i, (a, piece) in enumerate(chunks):
        until = (half - 1) * (i + 1) // len(chunks)
        lax.fori_loop(done, until, own_step, 0)
        done = until
        forward(a, piece)
    ret[mine, 0] = dot(hidden_rows(arr[mine, 0], wg[...], wu[...]), wd[...]).astype(BF16)

    for a, piece in chunks:
        for k in range(1, groups):
            forward_copy(a, piece, k).wait_recv()

    def far_step(i, c):
        p = peer(half - 1 - i)
        ybuf[p, 1] = dot(hidden_rows(arr[p, 1], fg[...], fu[...]), fd[...]).astype(BF16)
        return_copy(p, 1).start()
        return c

    lax.fori_loop(0, half - 1, far_step, 0)
    ret[mine, 1] = dot(hidden_rows(arr[mine, 1], fg[...], fu[...]), fd[...]).astype(BF16)

    combine(mine, 0)
    combine(mine, 1)
    for b in range(2):

        def combine_step(i, c):
            p = peer(half - 1 - i)
            return_wait(p, b)
            combine(p, b)
            return c

        lax.fori_loop(0, half - 1, combine_step, 0)
    out_ref[...] = acc[...].astype(BF16)

    def drain(i, c):
        p = peer(half - 1 - i)
        dispatch_copy(p).wait_send()
        return_copy(p, 0).wait_send()
        return_copy(p, 1).wait_send()
        return c

    lax.fori_loop(0, half - 1, drain, 0)
    for a, piece in chunks:
        weight_copy(a, piece).wait_send()
        for k in range(1, groups):
            forward_copy(a, piece, k).wait_send()


def on_device(tokens, norm_gain, routes, route_weights, expert_gate, expert_up, expert_down,
              shared_gate, shared_up, shared_down):
    rows, width = tokens.shape
    n, groups = lax.axis_size("ep"), lax.axis_size("grp")
    half = n // 2
    cap = -(-(5 * rows * routes.shape[1] // (4 * n)) // 8) * 8
    nchunk = 3 * PIECES
    nfwd = nchunk * max(1, groups - 1)
    vmem = lambda shape, kind=BF16: pltpu.VMEM(shape, kind)
    anyspec = pl.BlockSpec(memory_space=pl.ANY)
    vspec = pl.BlockSpec(memory_space=pltpu.VMEM)
    block = (half, 2, cap, width)
    return pl.pallas_call(
        functools.partial(kernel, n, groups, cap),
        out_shape=jax.ShapeDtypeStruct((rows, width), BF16),
        in_specs=[anyspec, vspec, vspec, vspec] + [anyspec] * 6,
        out_specs=vspec,
        scratch_shapes=[
            vmem((rows, width)), vmem((rows, width)), vmem((128, rows), F32), vmem((128, rows), F32),
            vmem(expert_gate.shape[1:]), vmem(expert_up.shape[1:]), vmem(expert_down.shape[1:]),
            vmem(expert_gate.shape[1:]), vmem(expert_up.shape[1:]), vmem(expert_down.shape[1:]),
            vmem(shared_gate.shape), vmem(shared_up.shape), vmem(shared_down.shape),
            vmem(block), vmem(block), vmem(block), vmem(block), vmem((rows, width), F32),
            pltpu.SemaphoreType.DMA((7,)),
            pltpu.SemaphoreType.DMA((nchunk,)), pltpu.SemaphoreType.DMA((nchunk,)),
            pltpu.SemaphoreType.DMA((nfwd,)), pltpu.SemaphoreType.DMA((nfwd,)),
            pltpu.SemaphoreType.DMA((half,)), pltpu.SemaphoreType.DMA((half,)),
            pltpu.SemaphoreType.DMA((half, 2)), pltpu.SemaphoreType.DMA((half, 2)),
        ],
        compiler_params=pltpu.CompilerParams(
            collective_id=0, has_side_effects=True, vmem_limit_bytes=60 * 1024 * 1024),
    )(tokens, norm_gain.reshape(1, width), routes, route_weights, expert_gate, expert_up,
      expert_down, shared_gate, shared_up, shared_down)


def solution(mesh):
    return jax.shard_map(
        on_device,
        mesh=mesh,
        in_specs=(
            P(("grp", "ep"), None),
            P(),
            P(("grp", "ep"), None),
            P(("grp", "ep"), None),
            P("ep", None, None),
            P("ep", None, None),
            P("ep", None, None),
            P(),
            P(),
            P(),
        ),
        out_specs=P(("grp", "ep"), None),
        check_vma=False,
    )
```

time: 174 us -> 113 us (0.65)
  the two profiles are of different devices: /device:TPU:13 before, /device:TPU:0 now
where the time goes in v1:
time: 113 us
  Pallas kernels  108 us (96%)
  local copies, waits for them, and re-layouts  4.59 us (4%)
    pallas_call x1, Pallas kernels, on_device(): pl.pallas_call(functools.partial(kernel, n, groups, cap), out_shape=jax.S...  108 us
    unnamed x5, local copies, waits for them, and re-layouts  4.59 us

profile of v1, /device:TPU:0, one launch (start us, length us, event | category | flops | bytes accessed | tf_op | source)
XLA Modules:
  0.0 112.9 jit_solution(3551235676965840155)
XLA Ops:
  0.0 0.0 copy-start
  0.0 1.5 %copy.11.routes_ref = s32[256,2]{1,0:T(8,128)} copy(s32[256,2]{0,1:T(2,128)} %param.12) | data formatting | bytes 4096 | tf_op args[2]
  1.5 0.0 copy-done
  1.5 0.8 copy.12.rw_ref
  2.3 108.3 %shard_map.100 = bf16[256,2048]{1,0:T(8,128)(2,1)} custom-call(bf16[256,2048]{1,0:T(8,128)(2,1)} %tokens_hbm.1, f32[1,2048]{1,0:T(1,128)} %bitcast.1, s32[256,2]{1,0:T(8,128)} %copy.11.routes_ref, f32[256,2]{1,0:T(8,128)} %copy.12.rw_ref, bf16[1,2048,256]{2,1,0:T(8,128)(2,1)} %eg_hbm.1, bf16[1,2048,256]{2,1,0:T(8,128)(2,1)} %eu_hbm.1, ...), custom_call_target="tpu_custom_call" | custom-call | tf_op jit(solution)/shard_map/pallas_call | solution.py:241
  110.5 2.3 %copy.14 = bf16[256,2048]{1,0:T(8,128)(2,1)} copy(bf16[256,2048]{1,0:T(8,128)(2,1)} %shard_map.100) | data formatting | bytes 2097152
Async XLA Ops:
  0.0 1.5 %copy-start = (f32[256,2]{0,1:T(2,128)S(1)}, f32[256,2]{0,1:T(2,128)}, u32[]{:S(2)}) copy-start(f32[256,2]{0,1:T(2,128)} %param.13) | copy-start | bytes 6148

commit v2 on v1

v2 whole, which is shorter than its diff:
```python
import functools

import jax
import jax.numpy as jnp
from jax import lax
from jax.experimental import pallas as pl
from jax.experimental.pallas import tpu as pltpu
from jax.sharding import PartitionSpec as P

BF16 = jnp.bfloat16
F32 = jnp.float32
PIECES = 2
SLABS = 4


def dot(a, b, dims=((1,), (0,))):
    return lax.dot_general(a, b, (dims, ((), ())), preferred_element_type=F32)


def hidden_rows(rows, w_gate, w_up):
    gate_part = dot(rows, w_gate)
    up_part = dot(rows, w_up)
    return (gate_part / (1.0 + jnp.exp(-gate_part)) * up_part).astype(BF16)


def kernel(
    n, groups, cap,
    tokens_hbm, gain_ref, routes_ref, rw_ref, eg_hbm, eu_hbm, ed_hbm, sg_hbm, su_hbm, sd_hbm,
    out_ref,
    tok, normed, place, scale, wg, wu, wd, fg, fu, fd, sg, su, sd, obuf, arr, ybuf, ret, acc, hid, pick,
    load_sem, wsend, wrecv, xsend, xrecv, dsend, drecv, rsend, rrecv,
):
    half = n // 2
    me = lax.axis_index("ep")
    grp = lax.axis_index("grp")
    base = (me // half) * half
    mine = me % half
    far = (me + half) % n
    rows = tok.shape[0]
    width = tok.shape[1]

    def peer(j):
        total, bit = 0, 1
        while bit < half:
            total = total + bit * (((mine // bit) % 2 + (j // bit) % 2) % 2)
            bit *= 2
        return total

    capp = ret.shape[2]
    if capp > cap:
        low = cap // 16 * 16
        ret[:, :, low:, :] = jnp.zeros((2, half, capp - low, width), BF16)
    barrier = pltpu.get_barrier_semaphore()

    def greet(i, c):
        pl.semaphore_signal(barrier, inc=1, device_id={"ep": base + peer(i)})
        return c

    lax.fori_loop(1, half, greet, 0)
    pl.semaphore_signal(barrier, inc=1, device_id={"ep": far})
    for k in range(1, groups):
        pl.semaphore_signal(barrier, inc=1, device_id={"grp": (grp + k) % groups})

    loads = [(tokens_hbm, tok), (eg_hbm.at[0], wg), (eu_hbm.at[0], wu), (ed_hbm.at[0], wd),
             (sg_hbm, sg), (su_hbm, su), (sd_hbm, sd)]
    loads = [pltpu.make_async_copy(a, b, load_sem.at[i]) for i, (a, b) in enumerate(loads)]
    for copy in loads:
        copy.start()

    slab = width // SLABS

    def region(group, a, piece):
        depth = (fg, fu, fd)[a].shape[0] // groups
        if a == 2:
            return pl.ds(pl.multiple_of(group * depth, depth), depth), pl.ds(piece * slab, slab)
        depth = depth // PIECES
        start = (group * PIECES + piece) * depth
        return pl.ds(pl.multiple_of(start, depth), depth), pl.ds(0, fg.shape[1])

    chunks = [(a, piece) for piece in range(PIECES) for a in range(2)]
    chunks += [(2, piece) for piece in range(SLABS)]

    def weight_copy(a, piece):
        src, dst = ((eg_hbm, fg), (eu_hbm, fu), (ed_hbm, fd))[a]
        at, i = region(grp, a, piece), chunks.index((a, piece))
        return pltpu.make_async_remote_copy(
            src_ref=src.at[0, at[0], at[1]], dst_ref=dst.at[at[0], at[1]],
            send_sem=wsend.at[i], recv_sem=wrecv.at[i], device_id={"ep": far})

    def forward_copy(a, piece, k):
        dst = (fg, fu, fd)[a]
        at = region(grp, a, piece)
        i = chunks.index((a, piece)) * max(1, groups - 1) + k - 1
        return pltpu.make_async_remote_copy(
            src_ref=dst.at[at[0], at[1]], dst_ref=dst.at[at[0], at[1]],
            send_sem=xsend.at[i], recv_sem=xrecv.at[i],
            device_id={"grp": (grp + k) % groups})

    pl.semaphore_wait(barrier, half - 1 + 1 + groups - 1)
    weight_copy(*chunks[0]).start()

    lane = lax.broadcasted_iota(jnp.int32, (rows, 128), 1)
    chosen = jnp.zeros((rows, 128), F32)
    weight = jnp.zeros((rows, 128), F32)
    for k in range(routes_ref.shape[1]):
        hit = lane == routes_ref[:, k:k + 1]
        chosen = chosen + jnp.where(hit, 1.0, 0.0)
        weight = weight + jnp.where(hit, rw_ref[:, k:k + 1], 0.0)
    chosen_t = chosen.T
    earlier = (lax.broadcasted_iota(jnp.int32, (rows, rows), 0)
               < lax.broadcasted_iota(jnp.int32, (rows, rows), 1))
    before = dot(chosen_t.astype(BF16), jnp.where(earlier, 1.0, 0.0).astype(BF16))
    place[...] = jnp.where(chosen_t > 0.5, before, -1.0)
    scale[...] = weight.T

    loads[0].wait()

    def norm_step(i, c):
        at = pl.ds(pl.multiple_of(i * 32, 32), 32)
        x = tok[at, :].astype(F32)
        factor = lax.rsqrt(jnp.mean(x * x, axis=-1, keepdims=True) + 1e-06)
        normed[at, :] = (x * factor * gain_ref[...]).astype(BF16)
        return c

    lax.fori_loop(0, rows // 32, norm_step, 0)
    slot = lax.broadcasted_iota(jnp.int32, (capp, rows), 0).astype(F32)
    slot = jnp.where(slot < cap, slot, -2.0)

    def gather(p):
        ours = slot == place[pl.ds(base + p, 1), :]
        theirs = slot == place[pl.ds((base + half) % n + p, 1), :]
        want = jnp.concatenate([jnp.where(ours, 1.0, 0.0), jnp.where(theirs, 1.0, 0.0)], axis=0)
        got = dot(want.astype(BF16), normed[...])
        return got[:capp].astype(BF16), got[capp:].astype(BF16)

    used = pl.ds(0, cap)

    def dispatch_copy(p):
        return pltpu.make_async_remote_copy(
            src_ref=obuf.at[:, p, used], dst_ref=arr.at[:, mine, used],
            send_sem=dsend.at[p], recv_sem=drecv.at[mine], device_id={"ep": base + p})

    def dispatch_wait(p):
        pltpu.make_async_remote_copy(
            src_ref=obuf.at[:, p, used], dst_ref=arr.at[:, p, used],
            send_sem=dsend.at[p], recv_sem=drecv.at[p], device_id={"ep": base + p}).wait_recv()

    def message(ref, p, m):
        if m == 0:
            return ref.at[0, p, used]
        return ref.at[1, p, used, pl.ds((m - 1) * slab, slab)]

    def return_copy(p, m):
        return pltpu.make_async_remote_copy(
            src_ref=message(ybuf, p, m), dst_ref=message(ret, mine, m),
            send_sem=rsend.at[p, m], recv_sem=rrecv.at[mine, m], device_id={"ep": base + p})

    def return_wait(p, m):
        pltpu.make_async_remote_copy(
            src_ref=message(ybuf, p, m), dst_ref=message(ret, p, m),
            send_sem=rsend.at[p, m], recv_sem=rrecv.at[p, m],
            device_id={"ep": base + p}).wait_recv()

    def dispatch_step(i, c):
        p = peer(half - 1 - i)
        first, second = gather(p)
        obuf[0, p] = first
        obuf[1, p] = second
        dispatch_copy(p).start()
        return c

    lax.fori_loop(0, half - 1, dispatch_step, 0)
    for a, piece in chunks[1:]:
        weight_copy(a, piece).start()
    first, second = gather(mine)
    arr[0, mine] = first
    arr[1, mine] = second

    for copy in loads[4:]:
        copy.wait()
    acc[...] = dot(hidden_rows(normed[...], sg[...], su[...]), sd[...])
    for copy in loads[1:4]:
        copy.wait()

    for b in range(2):
        for p in range(half):
            at = pl.ds((base + b * half) % n + p, 1)
            want = jnp.where(slot == place[at, :], scale[at, :], 0.0)
            pick[b, p * capp:(p + 1) * capp, :] = want.astype(BF16)

    def own_step(i, c):
        p = peer(i + 1)
        dispatch_wait(p)
        ybuf[0, p] = dot(hidden_rows(arr[0, p], wg[...], wu[...]), wd[...]).astype(BF16)
        return_copy(p, 0).start()
        return c

    def forward(a, piece):
        weight_copy(a, piece).wait_recv()
        for k in range(1, groups):
            forward_copy(a, piece, k).start()

    def forwarded(a, piece):
        for k in range(1, groups):
            forward_copy(a, piece, k).wait_recv()

    early = chunks[:-SLABS]
    done = 0
    for i, (a, piece) in enumerate(early):
        until = (half - 1) * (i + 1) // len(early)
        lax.fori_loop(done, until, own_step, 0)
        done = until
        forward(a, piece)
    own = dot(hidden_rows(arr[0, mine], wg[...], wu[...]), wd[...]).astype(BF16)
    ret[0, mine] = own

    for a, piece in early:
        forwarded(a, piece)
    hid[...] = hidden_rows(arr[1].reshape(half * capp, width), fg[...], fu[...])

    def far_slab(c):
        forwarded(2, c)
        cols = pl.ds(c * slab, slab)
        got = dot(hid[...], fd[:, cols]).astype(BF16)
        ybuf[1, :, :, cols] = got.reshape(half, capp, slab)

        def send(i, k):
            return_copy(peer(half - 1 - i), 1 + c).start()
            return k

        lax.fori_loop(0, half - 1, send, 0)
        local = pl.ds(pl.multiple_of(mine * capp, capp), capp)
        ret[1, mine, :, cols] = dot(hid[local, :], fd[:, cols]).astype(BF16)

    for c in range(SLABS):
        forward(2, c)
        if c > 0:
            far_slab(c - 1)
    far_slab(SLABS - 1)

    def arrive(m):
        def step(i, k):
            return_wait(peer(i + 1), m)
            return k

        lax.fori_loop(0, half - 1, step, 0)

    arrive(0)
    acc[...] += dot(pick[0], ret[0].reshape(half * capp, width), ((0,), (0,)))
    for c in range(SLABS):
        arrive(1 + c)
        cols = pl.ds(c * slab, slab)
        total = acc[:, cols] + dot(
            pick[1], ret[1, :, :, cols].reshape(half * capp, slab), ((0,), (0,)))
        out_ref[:, cols] = total.astype(BF16)

    def drain(i, c):
        p = peer(half - 1 - i)
        dispatch_copy(p).wait_send()
        for m in range(1 + SLABS):
            return_copy(p, m).wait_send()
        return c

    lax.fori_loop(0, half - 1, drain, 0)
    for a, piece in chunks:
        weight_copy(a, piece).wait_send()
        for k in range(1, groups):
            forward_copy(a, piece, k).wait_send()


def on_device(tokens, norm_gain, routes, route_weights, expert_gate, expert_up, expert_down,
              shared_gate, shared_up, shared_down):
    rows, width = tokens.shape
    n, groups = lax.axis_size("ep"), lax.axis_size("grp")
    half = n // 2
    cap = -(-(5 * rows * routes.shape[1] // (4 * n)) // 8) * 8
    nchunk = 2 * PIECES + SLABS
    nfwd = nchunk * max(1, groups - 1)
    vmem = lambda shape, kind=BF16: pltpu.VMEM(shape, kind)
    anyspec = pl.BlockSpec(memory_space=pl.ANY)
    vspec = pl.BlockSpec(memory_space=pltpu.VMEM)
    capp = -(-cap // 16) * 16
    block = (2, half, capp, width)
    return pl.pallas_call(
        functools.partial(kernel, n, groups, cap),
        out_shape=jax.ShapeDtypeStruct((rows, width), BF16),
        in_specs=[anyspec, vspec, vspec, vspec] + [anyspec] * 6,
        out_specs=vspec,
        scratch_shapes=[
            vmem((rows, width)), vmem((rows, width)), vmem((128, rows), F32), vmem((128, rows), F32),
            vmem(expert_gate.shape[1:]), vmem(expert_up.shape[1:]), vmem(expert_down.shape[1:]),
            vmem(expert_gate.shape[1:]), vmem(expert_up.shape[1:]), vmem(expert_down.shape[1:]),
            vmem(shared_gate.shape), vmem(shared_up.shape), vmem(shared_down.shape),
            vmem(block), vmem(block), vmem(block), vmem(block), vmem((rows, width), F32),
            vmem((half * capp, expert_gate.shape[2])), vmem((2, half * capp, rows)),
            pltpu.SemaphoreType.DMA((7,)),
            pltpu.SemaphoreType.DMA((nchunk,)), pltpu.SemaphoreType.DMA((nchunk,)),
            pltpu.SemaphoreType.DMA((nfwd,)), pltpu.SemaphoreType.DMA((nfwd,)),
            pltpu.SemaphoreType.DMA((half,)), pltpu.SemaphoreType.DMA((half,)),
            pltpu.SemaphoreType.DMA((half, 1 + SLABS)), pltpu.SemaphoreType.DMA((half, 1 + SLABS)),
        ],
        compiler_params=pltpu.CompilerParams(
            collective_id=0, has_side_effects=True, vmem_limit_bytes=60 * 1024 * 1024),
    )(tokens, norm_gain.reshape(1, width), routes, route_weights, expert_gate, expert_up,
      expert_down, shared_gate, shared_up, shared_down)


def solution(mesh):
    return jax.shard_map(
        on_device,
        mesh=mesh,
        in_specs=(
            P(("grp", "ep"), None),
            P(),
            P(("grp", "ep"), None),
            P(("grp", "ep"), None),
            P("ep", None, None),
            P("ep", None, None),
            P("ep", None, None),
            P(),
            P(),
            P(),
        ),
        out_specs=P(("grp", "ep"), None),
        check_vma=False,
    )
```

time: 113 us -> 107 us (0.947)
  Pallas kernels: 108 us -> 102 us
    pallas_call x1, Pallas kernels: 108 us -> 102 us  [on_device(): pl.pallas_call(functools.partial(kernel, n, groups, cap), out_shape=jax.S...]
where the time goes in v2:
time: 107 us
  Pallas kernels  102 us (95%)
  local copies, waits for them, and re-layouts  4.59 us (4%)
    pallas_call x1, Pallas kernels, on_device(): pl.pallas_call(functools.partial(kernel, n, groups, cap), out_shape=jax.S...  102 us
    unnamed x5, local copies, waits for them, and re-layouts  4.59 us

profile of v2, /device:TPU:0, one launch (start us, length us, event | category | flops | bytes accessed | tf_op | source)
XLA Modules:
  0.0 106.9 jit_solution(6315042401484751892)
XLA Ops:
  0.0 0.0 copy-start
  0.0 1.5 %copy.11.routes_ref = s32[256,2]{1,0:T(8,128)} copy(s32[256,2]{0,1:T(2,128)} %param.12) | data formatting | bytes 4096 | tf_op args[2]
  1.5 0.0 copy-done
  1.5 0.8 copy.12.rw_ref
  2.3 102.3 %shard_map.100 = bf16[256,2048]{1,0:T(8,128)(2,1)} custom-call(bf16[256,2048]{1,0:T(8,128)(2,1)} %tokens_hbm.1, f32[1,2048]{1,0:T(1,128)} %bitcast.1, s32[256,2]{1,0:T(8,128)} %copy.11.routes_ref, f32[256,2]{1,0:T(8,128)} %copy.12.rw_ref, bf16[1,2048,256]{2,1,0:T(8,128)(2,1)} %eg_hbm.1, bf16[1,2048,256]{2,1,0:T(8,128)(2,1)} %eu_hbm.1, ...), custom_call_target="tpu_custom_call" | custom-call | tf_op jit(solution)/shard_map/pallas_call | solution.py:284
  104.6 2.3 %copy.14 = bf16[256,2048]{1,0:T(8,128)(2,1)} copy(bf16[256,2048]{1,0:T(8,128)(2,1)} %shard_map.100) | data formatting | bytes 2097152
Async XLA Ops:
  0.0 1.5 %copy-start = (f32[256,2]{0,1:T(2,128)S(1)}, f32[256,2]{0,1:T(2,128)}, u32[]{:S(2)}) copy-start(f32[256,2]{0,1:T(2,128)} %param.13) | copy-start | bytes 6148

commit v3 on v2

--- a/solution.py
+++ b/solution.py
@@ -35,7 +35,7 @@
     grp = lax.axis_index("grp")
     base = (me // half) * half
     mine = me % half
-    far = (me + half) % n
+    far = (base + half) % n + (mine + half // 2) % half
     rows = tok.shape[0]
     width = tok.shape[1]
 
@@ -128,7 +128,7 @@
 
     def gather(p):
         ours = slot == place[pl.ds(base + p, 1), :]
-        theirs = slot == place[pl.ds((base + half) % n + p, 1), :]
+        theirs = slot == place[pl.ds((base + half) % n + (p + half // 2) % half, 1), :]
         want = jnp.concatenate([jnp.where(ours, 1.0, 0.0), jnp.where(theirs, 1.0, 0.0)], axis=0)
         got = dot(want.astype(BF16), normed[...])
         return got[:capp].astype(BF16), got[capp:].astype(BF16)
@@ -170,7 +170,7 @@
         return c
 
     lax.fori_loop(0, half - 1, dispatch_step, 0)
-    for a, piece in chunks[1:]:
+    for a, piece in chunks[1:-SLABS]:
         weight_copy(a, piece).start()
     first, second = gather(mine)
     arr[0, mine] = first
@@ -184,7 +184,7 @@
 
     for b in range(2):
         for p in range(half):
-            at = pl.ds((base + b * half) % n + p, 1)
+            at = pl.ds((base + b * half) % n + (p + b * (half // 2)) % half, 1)
             want = jnp.where(slot == place[at, :], scale[at, :], 0.0)
             pick[b, p * capp:(p + 1) * capp, :] = want.astype(BF16)
 
@@ -211,6 +211,7 @@
         lax.fori_loop(done, until, own_step, 0)
         done = until
         forward(a, piece)
+        weight_copy(*chunks[len(early) + i]).start()
     own = dot(hidden_rows(arr[0, mine], wg[...], wu[...]), wd[...]).astype(BF16)
     ret[0, mine] = own
 
@@ -229,8 +230,7 @@
             return k
 
         lax.fori_loop(0, half - 1, send, 0)
-        local = pl.ds(pl.multiple_of(mine * capp, capp), capp)
-        ret[1, mine, :, cols] = dot(hid[local, :], fd[:, cols]).astype(BF16)
+        ret[1, mine, :, cols] = ybuf[1, mine, :, cols]
 
     for c in range(SLABS):
         forward(2, c)
@@ -279,7 +279,7 @@
     vmem = lambda shape, kind=BF16: pltpu.VMEM(shape, kind)
     anyspec = pl.BlockSpec(memory_space=pl.ANY)
     vspec = pl.BlockSpec(memory_space=pltpu.VMEM)
-    capp = -(-cap // 16) * 16
+    capp = cap
     block = (2, half, capp, width)
     return pl.pallas_call(
         functools.partial(kernel, n, groups, cap),

time: 107 us -> 106 us (level)
  no operation moved by 1% of the time
where the time goes in v3:
time: 106 us
  Pallas kernels  102 us (96%)
  local copies, waits for them, and re-layouts  4.59 us (4%)
    pallas_call x1, Pallas kernels, on_device(): pl.pallas_call(functools.partial(kernel, n, groups, cap), out_shape=jax.S...  102 us
    unnamed x5, local copies, waits for them, and re-layouts  4.59 us

profile of v3, /device:TPU:0, one launch (start us, length us, event | category | flops | bytes accessed | tf_op | source)
XLA Modules:
  0.0 106.2 jit_solution(16841796632765357328)
XLA Ops:
  0.0 0.0 copy-start
  0.0 1.5 %copy.11.routes_ref = s32[256,2]{1,0:T(8,128)} copy(s32[256,2]{0,1:T(2,128)} %param.12) | data formatting | bytes 4096 | tf_op args[2]
  1.5 0.0 copy-done
  1.5 0.8 copy.12.rw_ref
  2.3 101.6 %shard_map.100 = bf16[256,2048]{1,0:T(8,128)(2,1)} custom-call(bf16[256,2048]{1,0:T(8,128)(2,1)} %tokens_hbm.1, f32[1,2048]{1,0:T(1,128)} %bitcast.1, s32[256,2]{1,0:T(8,128)} %copy.11.routes_ref, f32[256,2]{1,0:T(8,128)} %copy.12.rw_ref, bf16[1,2048,256]{2,1,0:T(8,128)(2,1)} %eg_hbm.1, bf16[1,2048,256]{2,1,0:T(8,128)(2,1)} %eu_hbm.1, ...), custom_call_target="tpu_custom_call" | custom-call | tf_op jit(solution)/shard_map/pallas_call | solution.py:284
  103.9 2.3 %copy.14 = bf16[256,2048]{1,0:T(8,128)(2,1)} copy(bf16[256,2048]{1,0:T(8,128)(2,1)} %shard_map.100) | data formatting | bytes 2097152
Async XLA Ops:
  0.0 1.5 %copy-start = (f32[256,2]{0,1:T(2,128)S(1)}, f32[256,2]{0,1:T(2,128)}, u32[]{:S(2)}) copy-start(f32[256,2]{0,1:T(2,128)} %param.13) | copy-start | bytes 6148

commit v4 on v3

--- a/solution.py
+++ b/solution.py
@@ -64,8 +64,7 @@
     loads = [(tokens_hbm, tok), (eg_hbm.at[0], wg), (eu_hbm.at[0], wu), (ed_hbm.at[0], wd),
              (sg_hbm, sg), (su_hbm, su), (sd_hbm, sd)]
     loads = [pltpu.make_async_copy(a, b, load_sem.at[i]) for i, (a, b) in enumerate(loads)]
-    for copy in loads:
-        copy.start()
+    loads[0].start()
 
     slab = width // SLABS
 
@@ -114,6 +113,8 @@
     scale[...] = weight.T
 
     loads[0].wait()
+    for copy in loads[1:]:
+        copy.start()
 
     def norm_step(i, c):
         at = pl.ds(pl.multiple_of(i * 32, 32), 32)
@@ -189,7 +190,7 @@
             pick[b, p * capp:(p + 1) * capp, :] = want.astype(BF16)
 
     def own_step(i, c):
-        p = peer(i + 1)
+        p = peer((i + half // 2 - 1) % (half - 1) + 1)
         dispatch_wait(p)
         ybuf[0, p] = dot(hidden_rows(arr[0, p], wg[...], wu[...]), wd[...]).astype(BF16)
         return_copy(p, 0).start()

time: 106 us -> 106 us (level)
  no operation moved by 1% of the time
where the time goes in v4:
time: 106 us
  Pallas kernels  102 us (96%)
  local copies, waits for them, and re-layouts  4.59 us (4%)
    pallas_call x1, Pallas kernels, on_device(): pl.pallas_call(functools.partial(kernel, n, groups, cap), out_shape=jax.S...  102 us
    unnamed x5, local copies, waits for them, and re-layouts  4.59 us

profile of v4, /device:TPU:0, one launch (start us, length us, event | category | flops | bytes accessed | tf_op | source)
XLA Modules:
  0.0 106.2 jit_solution(9741662490169713132)
XLA Ops:
  0.0 0.0 copy-start
  0.0 1.5 %copy.11.routes_ref = s32[256,2]{1,0:T(8,128)} copy(s32[256,2]{0,1:T(2,128)} %param.12) | data formatting | bytes 4096 | tf_op args[2]
  1.5 0.0 copy-done
  1.5 0.8 copy.12.rw_ref
  2.3 101.6 %shard_map.100 = bf16[256,2048]{1,0:T(8,128)(2,1)} custom-call(bf16[256,2048]{1,0:T(8,128)(2,1)} %tokens_hbm.1, f32[1,2048]{1,0:T(1,128)} %bitcast.1, s32[256,2]{1,0:T(8,128)} %copy.11.routes_ref, f32[256,2]{1,0:T(8,128)} %copy.12.rw_ref, bf16[1,2048,256]{2,1,0:T(8,128)(2,1)} %eg_hbm.1, bf16[1,2048,256]{2,1,0:T(8,128)(2,1)} %eu_hbm.1, ...), custom_call_target="tpu_custom_call" | custom-call | tf_op jit(solution)/shard_map/pallas_call | solution.py:285
  103.9 2.3 %copy.14 = bf16[256,2048]{1,0:T(8,128)(2,1)} copy(bf16[256,2048]{1,0:T(8,128)(2,1)} %shard_map.100) | data formatting | bytes 2097152
Async XLA Ops:
  0.0 1.5 %copy-start = (f32[256,2]{0,1:T(2,128)S(1)}, f32[256,2]{0,1:T(2,128)}, u32[]{:S(2)}) copy-start(f32[256,2]{0,1:T(2,128)} %param.13) | copy-start | bytes 6148
